TPU v7x, 32 devices: a whole 2x2x4 slice. The times are simulated.
32 devices in a mesh: grp: 2 (over y), kv: 4 (over z), tp: 4 (over x, core).
Axes of the slice: x: 2, y: 2, z: 4, core: 2. Of those that a mesh axis runs over, the one named last changes fastest.
Arguments:
- tokens: bfloat16 [160, 4096], P('grp', ('kv', 'tp')), parts along dimension 0, may hold values from -65 to 65
- lengths: int32 [160], P(('grp', 'kv')), parts along dimension 0, may hold values from 1 to 16384, 327680 in all
- memory: float32 [160, 16, 128, 128], P(('grp', 'kv'), 'tp'), parts along dimension 0, may hold values from -6 to 6
- norm_attn: bfloat16 [4096], P('kv'), may hold values from 0.099609375 to 1.8984375
- w_query: bfloat16 [4096, 2048], P('kv', 'tp'), may hold values from -0.09375 to 0.09375
- w_key: bfloat16 [4096, 2048], P('kv', 'tp'), may hold values from -0.09375 to 0.09375
- w_value: bfloat16 [4096, 2048], P('kv', 'tp'), may hold values from -0.09375 to 0.09375
- w_gate: bfloat16 [4096, 2048], P('kv', 'tp'), may hold values from -0.09375 to 0.09375
- head_gain: bfloat16 [2048], P('tp'), may hold values from 0.099609375 to 1.8984375
- w_out: bfloat16 [2048, 4096], P('tp', 'kv'), may hold values from -0.1875 to 0.1875
- norm_mlp: bfloat16 [4096], P('kv'), may hold values from 0.099609375 to 1.8984375
- w_gate_mlp: bfloat16 [4096, 14336], P('kv', 'tp'), may hold values from -0.09375 to 0.09375
- w_up: bfloat16 [4096, 14336], P('kv', 'tp'), may hold values from -0.09375 to 0.09375
- w_down: bfloat16 [14336, 4096], P('tp', 'kv'), may hold values from -0.0625 to 0.0625
Outputs:
- result: bfloat16 [160, 4096], P('grp', ('kv', 'tp')), parts along dimension 0
- new_memory: float32 [160, 16, 128, 128], P(('grp', 'kv'), 'tp'), parts along dimension 0
There are 2 independent parts, one for each index of `grp`. A program takes and returns all parts, laid end to end along the dimension named above; an argument that names none is the same for every part. Nothing has to cross between parts.
Inputs may be any that keep to these rules, and one draw needn't show every extreme that they name: Within each part along grp the lengths sum to 327680 and the longest is exactly 16384.
All inputs are finite; a program needn't handle non-finite values. No bound on the sum of `lengths` on one device may be relied on, other than what follows from the above.
Results may differ from a plain program's by a relative error of at most 0.025.
Values may be sent and summed in bfloat16 or wider, within the bound.
A program may use at most 64 MiB of HBM per device.

v0:
```python
import jax
import jax.numpy as jnp
from jax import lax
from jax.sharding import PartitionSpec as P

D = 4096
HEADS = 16


epsilon = 1e-06


def rotate(values, position):
    half_width = values.shape[-1] // 2
    inverse = 10000.0 ** (-jnp.arange(half_width, dtype=jnp.float32) / half_width)
    angles = position[:, None] * inverse[None, :]
    cosine = jnp.cos(angles)[:, None, :]
    sine = jnp.sin(angles)[:, None, :]
    first = values[..., :half_width]
    second = values[..., half_width:]
    return jnp.concatenate(
        [first * cosine - second * sine, second * cosine + first * sine], axis=-1
    )


def head_decay(head_index):
    exponent = -5.0 - head_index.astype(jnp.float32) * (7.0 / max(HEADS - 1, 1))
    return 1.0 - jnp.exp2(exponent)


def retain(memory, queries, key_rows, value_rows, gate_rows, head_gain, decay_rate):
    new_memory = (
        decay_rate[None, :, None, None] * memory
        + key_rows[:, :, :, None] * value_rows[:, :, None, :]
    )
    readout = jnp.einsum(
        "bhd,bhde->bhe",
        queries * queries.shape[-1] ** (-0.5),
        new_memory,
        precision=lax.Precision.HIGHEST,
    )
    centred = readout - jnp.mean(readout, axis=-1, keepdims=True)
    normed = centred * lax.rsqrt(jnp.mean(centred * centred, axis=-1, keepdims=True) + epsilon)
    normed = normed.reshape(readout.shape[0], -1) * head_gain.astype(jnp.float32)
    return (new_memory, (normed * jax.nn.silu(gate_rows)).astype(jnp.bfloat16))


def per_device(
    tokens,
    lengths,
    memory,
    norm_attn,
    w_query,
    w_key,
    w_value,
    w_gate,
    head_gain,
    w_out,
    norm_mlp,
    w_gate_mlp,
    w_up,
    w_down,
):
    own_count = memory.shape[0]
    heads_local = memory.shape[1]
    head_size = memory.shape[2]
    width_local = w_query.shape[1]
    gathered = lax.all_gather(tokens, "tp", axis=1, tiled=True)
    tok_float = gathered.astype(jnp.float32)
    square_part = jnp.sum(tok_float * tok_float, axis=1)
    scaled = (tok_float * norm_attn.astype(jnp.float32)).astype(jnp.bfloat16)
    own_start = lax.axis_index("kv") * own_count
    square_total = lax.psum(square_part, "kv")
    own_squares = lax.dynamic_slice_in_dim(square_total, own_start, own_count, 0)
    block_rows = scaled
    projected = lax.psum_scatter(
        jnp.concatenate(
            [
                jnp.dot(block_rows, weight, preferred_element_type=jnp.float32)
                for weight in (w_query, w_key, w_value, w_gate)
            ],
            axis=1,
        ).astype(jnp.bfloat16),
        "kv",
        scatter_dimension=0,
        tiled=True,
    ).astype(jnp.float32)
    projected = projected * lax.rsqrt(own_squares / D + epsilon)[:, None]
    position = lengths.astype(jnp.float32)
    queries = rotate(
        projected[:, :width_local].reshape(own_count, heads_local, head_size), position
    )
    key_rows = rotate(
        projected[:, width_local : 2 * width_local].reshape(own_count, heads_local, head_size),
        position,
    )
    value_rows = projected[:, 2 * width_local : 3 * width_local].reshape(
        own_count, heads_local, head_size
    )
    gate_rows = projected[:, 3 * width_local :]
    decay_rate = head_decay(lax.axis_index("tp") * heads_local + jnp.arange(heads_local))
    new_memory, mixed = retain(
        memory, queries, key_rows, value_rows, gate_rows, head_gain, decay_rate
    )
    attn_part = jnp.dot(
        lax.all_gather(mixed, "kv", axis=0, tiled=True), w_out, preferred_element_type=jnp.float32
    )
    attn_total = lax.psum_scatter(
        attn_part.astype(jnp.bfloat16), "tp", scatter_dimension=1, tiled=True
    ).astype(jnp.float32)
    middle = (tokens.astype(jnp.float32) + attn_total).astype(jnp.bfloat16)
    mid_float = middle.astype(jnp.float32)
    gathered_mid = lax.all_gather(middle, "tp", axis=1, tiled=True)
    gathered_float = gathered_mid.astype(jnp.float32)
    mid_squares = jnp.sum(gathered_float * gathered_float, axis=1)
    scaled_mid = (gathered_float * norm_mlp.astype(jnp.float32)).astype(jnp.bfloat16)
    ff_local = w_up.shape[1]
    pieces = 1
    span = scaled_mid.shape[0] // pieces
    own_span = span // lax.axis_size("kv")
    span_start = lax.axis_index("kv") * own_span
    square_sums = lax.psum(mid_squares, "kv")
    span_squares = lax.dynamic_slice_in_dim(square_sums, span_start, own_span, 0)
    block_rows = scaled_mid
    both_terms = lax.psum_scatter(
        jnp.concatenate(
            [
                jnp.dot(block_rows, w_gate_mlp, preferred_element_type=jnp.float32),
                jnp.dot(block_rows, w_up, preferred_element_type=jnp.float32),
            ],
            axis=1,
        ).astype(jnp.bfloat16),
        "kv",
        scatter_dimension=0,
        tiled=True,
    ).astype(jnp.float32)
    inv_mlp = lax.rsqrt(span_squares / D + epsilon)[:, None]
    gate_mlp = inv_mlp * both_terms[:, :ff_local]
    up_rows = inv_mlp * both_terms[:, ff_local:]
    hidden = (jax.nn.silu(gate_mlp) * up_rows).astype(jnp.bfloat16)
    partial_mlp = jnp.dot(
        lax.all_gather(hidden, "kv", axis=0, tiled=True), w_down, preferred_element_type=jnp.float32
    )
    results = lax.psum_scatter(
        partial_mlp.astype(jnp.bfloat16), "tp", scatter_dimension=1, tiled=True
    ).astype(jnp.float32)
    return ((mid_float + results).astype(jnp.bfloat16), new_memory)


def solution(mesh):
    in_specs = (
        P("grp", ("kv", "tp")),
        P(("grp", "kv")),
        P(("grp", "kv"), "tp", None, None),
        P("kv"),
        P("kv", "tp"),
        P("kv", "tp"),
        P("kv", "tp"),
        P("kv", "tp"),
        P("tp"),
        P("tp", "kv"),
        P("kv"),
        P("kv", "tp"),
        P("kv", "tp"),
        P("tp", "kv"),
    )
    out_specs = (P("grp", ("kv", "tp")), P(("grp", "kv"), "tp", None, None))
    return jax.shard_map(
        per_device, mesh=mesh, in_specs=in_specs, out_specs=out_specs, check_vma=False
    )
```

profile of v0, /device:TPU:0, one launch (start us, length us, event | category | flops | bytes accessed | tf_op | source)
XLA Modules:
  0.0 204.4 jit_solution(17068446962477856953)
XLA Ops:
  7.2 0.0 copy-start
  7.2 0.0 copy-start.5
  7.2 0.0 copy-start.6
  7.2 0.0 copy-start.4
  7.2 0.0 reduce-scatter.7.cloned.1.call-start
  7.3 0.8 convert_element_type.71
  8.0 6.9 %all_gather.12 = bf16[80,1024]{1,0:T(8,128)(2,1)S(1)} all-gather(bf16[80,256]{1,0:T(8,128)(2,1)} %param.14), channel_id=1, replica_groups=mesh['grp'=2,'kv'=4,'tp'=4] {'tp'}, dimensions={1}, use_global_device_ids=true | all-gather | bytes 204800 | tf_op jit(solution)/shard_map/all_gather | solution.py:68
  14.9 1.5 convolution_convert_fusion.6
  16.4 1.5 convolution_convert_fusion.5
  17.9 1.5 convolution_convert_fusion.4
  19.5 1.5 convolution_convert_fusion.7
  21.0 16.8 %fusion = bf16[24,2048]{1,0:T(8,128)(2,1)S(1)} fusion(bf16[80,2048]{1,0:T(8,128)(2,1)S(1)} %pad_maximum_fusion.1), kind=kCustom, calls=%all-reduce-scatter | all-reduce-scatter fusion | flops 196609 | bytes 426496
  37.8 2.4 %collective-permute-start = (bf16[12,2048]{1,0:T(8,128)(2,1)S(1)}, bf16[12,2048]{1,0:T(8,128)(2,1)S(1)}, u32[]{:S(2)}, u32[]{:S(2)}) collective-permute-start(bf16[12,2048]{1,0:T(8,128)(2,1)S(1)} %slice.50), channel_id=1, source_target_pairs={{0,4},{4,8},{8,12},{1,5},{5,9},{9,13},{2,6},{6,10},{10,14},{3,7},{... | collective-permute-start | bytes 147464
  40.2 0.1 fusion.5
  40.3 0.0 copy-done.6
  40.4 8.4 %psum.14 = f32[80]{0:T(128)S(1)} all-reduce(f32[80]{0:T(128)S(1)} %fusion.5), channel_id=1, replica_groups=mesh['grp'=2,'kv'=4,'tp'=4] {'kv'}, use_global_device_ids=true, to_apply=%region_2.0 | all-reduce | flops 80 | bytes 640 | tf_op jit(solution)/shard_map/psum | solution.py:73
  48.8 0.1 multiply_cosine_fusion
  48.9 0.1 add_rsqrt_fusion.2
  49.0 0.0 copy-done.4
  49.0 0.0 copy-done.5
  49.0 0.6 dynamic-slice.6
  50.3 0.0 collective-permute-done
  50.3 0.2 concatenate.18
  50.5 0.1 convert_multiply_fusion.4
  50.7 0.1 multiply_subtract_fusion
  50.8 0.1 maximum_multiply_fusion
  50.9 4.0 %multiply_add_fusion = f32[20,4,128,128]{3,2,1,0:T(8,128)S(1)} fusion(f32[20,4,128,128]{3,2,1,0:T(8,128)} %param.16, f32[20,4,128]{2,1,0:T(4,128)S(1)} %mul.225, f32[20,4,128]{2,1,0:T(4,128)S(1)} %get-tuple-element.14, f32[4]{0:T(128)S(1)} %exponential_subtract_fusion), kind=kLoop, calls=%fused_computation | loop fusion | flops 3932160 | bytes 10567696 | tf_op jit(solution)/shard_map/add | solution.py:33
  55.0 0.0 copy-start.1
  55.0 0.0 copy-start.3
  55.0 0.0 copy-start.2
  55.0 2.3 %copy-done.1 = f32[20,4,128,128]{3,2,1,0:T(8,128)} copy-done((f32[20,4,128,128]{3,2,1,0:T(8,128)}, f32[20,4,128,128]{3,2,1,0:T(8,128)S(1)}, u32[]{:S(2)}) %copy-start.1) | copy-done | bytes 5242904
  57.3 4.5 %fusion.17 = f32[20,4,1,128]{3,2,1,0:T(1,128)S(1)} fusion(f32[20,4,128,1]{2,3,1,0:T(1,128)S(1)} %bitcast.34, f32[20,4,128,128]{3,2,1,0:T(8,128)S(1)} %multiply_add_fusion), kind=kOutput, calls=%fused_computation.47 | convolution fusion | flops 15728640 | bytes 5324800 | tf_op jit(solution)/shard_map/bhd,bhde->bhe/dot_general | solution.py:36
  61.9 0.1 reduce_sum.37
  62.0 0.2 multiply_reduce_fusion
  62.2 0.1 subtract_multiply_fusion
  62.4 13.4 %all-gather = bf16[4,20,512]{2,1,0:T(8,128)(2,1)S(1)} all-gather(bf16[1,20,512]{2,1,0:T(8,128)(2,1)S(1)} %fusion.15), channel_id=1, replica_groups=mesh['grp'=2,'kv'=4,'tp'=4] {'kv'}, dimensions={0}, use_global_device_ids=true | all-gather | bytes 102400 | tf_op jit(solution)/shard_map/all_gather | solution.py:106
  75.7 0.0 copy-done
  75.7 1.0 convolution_convert_fusion.2
  76.7 0.0 reduce-scatter.7.cloned.1.call-update
  76.7 0.0 reduce-scatter.9.cloned.1.call-start
  76.8 0.0 copy-done.3
  76.8 19.5 %reduce-scatter.7.cloned.1.call-done = bf16[80,256]{1,0:T(8,128)(2,1)} async-done(((bf16[80,1024]{1,0:T(8,128)(2,1)}), bf16[80,256]{1,0:T(8,128)(2,1)}) %reduce-scatter.7.cloned.1.call-update) | async-done | bytes 40976 | tf_op jit(solution)/shard_map/reduce_scatter | solution.py:108
  96.3 0.0 copy-done.2
  96.3 0.8 add_convert_fusion.1
  97.1 5.5 %all_gather.14 = bf16[80,1024]{1,0:T(8,128)(2,1)S(1)} all-gather(bf16[80,256]{1,0:T(8,128)(2,1)S(1)} %add_convert_fusion.1), channel_id=1, replica_groups=mesh['grp'=2,'kv'=4,'tp'=4] {'tp'}, dimensions={1}, use_global_device_ids=true | all-gather | bytes 204800 | tf_op jit(solution)/shard_map/all_gather | solution.py:113
  102.6 4.4 %convolution_convert_fusion = bf16[80,3584]{1,0:T(8,128)(2,1)S(1)} fusion(bf16[1024,3584]{1,0:T(8,128)(2,1)} %param.26, bf16[80,1024]{1,0:T(8,128)(2,1)S(1)} %all_gather.14, f32[1024]{0:T(1024)S(1)} %convert_element_type.83), kind=kOutput, calls=%fused_computation.1 | convolution fusion | flops 587735040 | bytes 8081408 | tf_op jit(solution)/shard_map/dot_general | solution.py:129
  107.1 4.4 %convolution_convert_fusion.1 = bf16[80,3584]{1,0:T(8,128)(2,1)S(1)} fusion(bf16[1024,3584]{1,0:T(8,128)(2,1)} %param.25, bf16[80,1024]{1,0:T(8,128)(2,1)S(1)} %all_gather.14, f32[1024]{0:T(1024)S(1)} %convert_element_type.83), kind=kOutput, calls=%fused_computation.2 | convolution fusion | flops 587735040 | bytes 8081408 | tf_op jit(solution)/shard_map/dot_general | solution.py:128
  111.5 0.1 pad_maximum_fusion
  111.6 31.3 %fusion.1 = bf16[24,7168]{1,0:T(8,128)(2,1)S(1)} fusion(bf16[80,7168]{1,0:T(8,128)(2,1)S(1)} %pad_maximum_fusion), kind=kCustom, calls=%all-reduce-scatter.1 | all-reduce-scatter fusion | flops 688129 | bytes 1491456
  142.9 0.1 slice.51
  142.9 1.3 collective-permute-start.1
  144.3 0.1 fusion.6
  144.4 10.1 %psum.15 = f32[80]{0:T(128)S(1)} all-reduce(f32[80]{0:T(128)S(1)} %fusion.6), channel_id=1, replica_groups=mesh['grp'=2,'kv'=4,'tp'=4] {'kv'}, use_global_device_ids=true, to_apply=%region_7.8 | all-reduce | flops 80 | bytes 640 | tf_op jit(solution)/shard_map/psum | solution.py:122
  154.5 0.1 add_rsqrt_fusion.1
  154.6 0.0 collective-permute-done.1
  154.6 2.4 %concatenate.19 = bf16[36,7168]{1,0:T(8,128)(2,1)S(1)} concatenate(bf16[12,7168]{1,0:T(8,128)(2,1)S(1)} %collective-permute-done.1, bf16[24,7168]{1,0:T(8,128)(2,1)S(1)} %fusion.1), dimensions={0} | concatenate | bytes 1032192
  157.1 0.1 dynamic-slice_convert_fusion
  157.1 0.2 fusion.8
  157.3 15.4 %all-gather.1 = bf16[4,20,3584]{2,1,0:T(8,128)(2,1)S(1)} all-gather(bf16[1,20,3584]{2,1,0:T(8,128)(2,1)S(1)} %fusion.8), channel_id=1, replica_groups=mesh['grp'=2,'kv'=4,'tp'=4] {'kv'}, dimensions={0}, use_global_device_ids=true | all-gather | bytes 716800 | tf_op jit(solution)/shard_map/all_gather | solution.py:142
  172.7 0.1 reshape.99
  172.9 5.1 %convolution_convert_fusion.3 = bf16[80,1024]{1,0:T(8,128)(2,1)} fusion(bf16[80,3584]{1,0:T(8,128)(2,1)S(1)} %reshape.99, bf16[3584,1024]{1,0:T(8,128)(2,1)} %param.27), kind=kOutput, calls=%fused_computation.4 | convolution fusion | flops 587284480 | bytes 8077312 | tf_op jit(solution)/shard_map/dot_general | solution.py:141
  178.0 0.0 reduce-scatter.9.cloned.1.call-update
  178.0 18.2 %reduce-scatter.9.cloned.1.call-done = bf16[80,256]{1,0:T(8,128)(2,1)} async-done(((bf16[80,1024]{1,0:T(8,128)(2,1)}), bf16[80,256]{1,0:T(8,128)(2,1)}) %reduce-scatter.9.cloned.1.call-update) | async-done | bytes 40976 | tf_op jit(solution)/shard_map/reduce_scatter | solution.py:144
  196.2 1.4 add_convert_fusion
  (17 shorter events, 0.2 us)
Async XLA Ops:
  7.2 68.6 %copy-start = (bf16[512,1024]{1,0:T(8,128)(2,1)S(1)}, bf16[512,1024]{1,0:T(8,128)(2,1)}, u32[]{:S(2)}) copy-start(bf16[512,1024]{1,0:T(8,128)(2,1)} %param.23) | copy-start | bytes 3145732
  7.2 41.9 %copy-start.5 = (u32[32]{0:T(128)S(1)}, u32[32]{0:T(128)}, u32[]{:S(2)}) copy-start(u32[32]{0:T(128)} %constant.51) | copy-start | bytes 388
  7.2 33.2 %copy-start.6 = (s32[20]{0:T(128)S(1)}, s32[20]{0:T(128)}, u32[]{:S(2)}) copy-start(s32[20]{0:T(128)} %param.15) | copy-start | bytes 244
  7.2 41.8 %copy-start.4 = (bf16[512]{0:T(512)(128)(2,1)S(1)}, bf16[512]{0:T(512)(128)(2,1)}, u32[]{:S(2)}) copy-start(bf16[512]{0:T(512)(128)(2,1)} %param.22) | copy-start | bytes 3076
  7.2 89.1 %reduce-scatter.7.cloned.1.call-start = ((), (), s32[]{:S(2)}) async-start(), calls=%async_computation.2 | async-start | bytes 204800 | tf_op jit(solution)/shard_map/reduce_scatter | solution.py:108
  37.8 12.5 %collective-permute-start = (bf16[12,2048]{1,0:T(8,128)(2,1)S(1)}, bf16[12,2048]{1,0:T(8,128)(2,1)S(1)}, u32[]{:S(2)}, u32[]{:S(2)}) collective-permute-start(bf16[12,2048]{1,0:T(8,128)(2,1)S(1)} %slice.50), channel_id=1, source_target_pairs={{0,4},{4,8},{8,12},{1,5},{5,9},{9,13},{2,6},{6,10},{10,14},{3,7},{... | collective-permute-start | bytes 147464
  55.0 2.4 %copy-start.1 = (f32[20,4,128,128]{3,2,1,0:T(8,128)}, f32[20,4,128,128]{3,2,1,0:T(8,128)S(1)}, u32[]{:S(2)}) copy-start(f32[20,4,128,128]{3,2,1,0:T(8,128)S(1)} %multiply_add_fusion) | copy-start | bytes 15728644
  55.0 21.8 %copy-start.3 = (bf16[1024]{0:T(1024)(128)(2,1)S(1)}, bf16[1024]{0:T(1024)(128)(2,1)}, u32[]{:S(2)}) copy-start(bf16[1024]{0:T(1024)(128)(2,1)} %param.24) | copy-start | bytes 6148
  55.0 41.3 %copy-start.2 = (bf16[80,256]{1,0:T(8,128)(2,1)S(1)}, bf16[80,256]{1,0:T(8,128)(2,1)}, u32[]{:S(2)}) copy-start(bf16[80,256]{1,0:T(8,128)(2,1)} %param.14) | copy-start | bytes 122884
  76.7 119.4 %reduce-scatter.9.cloned.1.call-start = ((), (), s32[]{:S(2)}) async-start(), calls=%async_computation.3 | async-start | bytes 204800 | tf_op jit(solution)/shard_map/reduce_scatter | solution.py:144
  142.9 11.7 %collective-permute-start.1 = (bf16[12,7168]{1,0:T(8,128)(2,1)S(1)}, bf16[12,7168]{1,0:T(8,128)(2,1)S(1)}, u32[]{:S(2)}, u32[]{:S(2)}) collective-permute-start(bf16[12,7168]{1,0:T(8,128)(2,1)S(1)} %slice.51), channel_id=1, source_target_pairs={{0,4},{4,8},{8,12},{1,5},{5,9},{9,13},{2,6},{6,10},{10,14},{3,7},{... | collective-permute-start | bytes 516104
Sparse Core Ops, SparseCore 0:
  76.9 19.4 reduce-scatter.6
  178.1 17.9 reduce-scatter.8
where the time goes:
time: 205 us; the launch traced here: 204 us
  blocking collectives  108 us (53%)
  waiting for transfers between devices  37.7 us (18%)
  matrix products  25.6 us (12%)
  between operations  15.1 us (7%)
  other arithmetic  8.66 us (4%)
  local copies, waits for them, and re-layouts  5.9 us (3%)
  starting transfers between devices  3.75 us (2%)
    unnamed x2, blocking collectives  48 us
    reduce_scatter x1, waiting for transfers between devices, per_device(): lax.psum_scatter(attn_part.astype(jnp.bfloat16), 'tp', scatter_dimension=...  19.5 us
    reduce_scatter x1, waiting for transfers between devices, per_device(): lax.psum_scatter(partial_mlp.astype(jnp.bfloat16), 'tp', scatter_dimensio...  18.2 us
    all_gather x1, blocking collectives, per_device(): lax.all_gather(hidden, 'kv', axis=0, tiled=True)  15.4 us
    all_gather x1, blocking collectives, per_device(): lax.all_gather(mixed, 'kv', axis=0, tiled=True)  13.4 us
    psum x1, blocking collectives, per_device(): square_sums = lax.psum(mid_squares, 'kv')  10.1 us
    psum x1, blocking collectives, per_device(): square_total = lax.psum(square_part, 'kv')  8.45 us
    all_gather x1, blocking collectives, per_device(): gathered = lax.all_gather(tokens, 'tp', axis=1, tiled=True)  6.88 us
  transfers between devices with their start and end apart: 4, of which 2 were waited for; matrix products, arithmetic and copies ran while one was open for 1% of the time, Pallas kernels for 0%

commit v1 on v0

v1 whole, which is shorter than its diff:
```python
import functools

import jax
import jax.numpy as jnp
from jax import lax
from jax.experimental import pallas as pl
from jax.experimental.pallas import tpu as pltpu
from jax.sharding import PartitionSpec as P

HEADS = 16
EPS = 1e-06
F32 = jnp.float32
BF16 = jnp.bfloat16
MESH = pl.DeviceIdType.MESH


def head_decay(head_index):
    exponent = -5.0 - head_index.astype(F32) * (7.0 / max(HEADS - 1, 1))
    return 1.0 - jnp.exp2(exponent)


def dot(a, b):
    return jnp.dot(a, b, preferred_element_type=F32)


def chunk_width(ff_local):
    return 512 if ff_local % 512 == 0 else 128


def start_all(axis, n, me, src_of, dst, ssem, rsem):
    copies = []
    for d in range(1, n):
        other = lax.rem(me + d, n)
        copy = pltpu.make_async_remote_copy(
            src_ref=src_of(other),
            dst_ref=dst.at[me],
            send_sem=ssem.at[d - 1],
            recv_sem=rsem.at[me],
            device_id={axis: other},
            device_id_type=MESH,
        )
        copy.start()
        copies.append(copy)
    return copies


def wait_all(axis, n, me, dst, ssem, rsem):
    for d in range(1, n):
        other = lax.rem(me + d, n)
        pltpu.make_async_remote_copy(
            src_ref=dst.at[other],
            dst_ref=dst.at[other],
            send_sem=ssem.at[d - 1],
            recv_sem=rsem.at[other],
            device_id={axis: other},
            device_id_type=MESH,
        ).wait_recv()


def spread(width, total, start):
    rows = lax.broadcasted_iota(jnp.int32, (width, total), 0)
    cols = lax.broadcasted_iota(jnp.int32, (width, total), 1)
    return jnp.where(rows + start == cols, 1.0, 0.0).astype(BF16)


def pick(width, total, start):
    rows = lax.broadcasted_iota(jnp.int32, (total, width), 0)
    cols = lax.broadcasted_iota(jnp.int32, (total, width), 1)
    return jnp.where(rows == cols + start, 1.0, 0.0).astype(BF16)


def joined(blocks, dt, tp):
    if dt % 128 == 0:
        return jnp.concatenate([blocks[j].astype(F32) for j in range(tp)], axis=1)
    total = dot(blocks[0], spread(dt, dt * tp, 0))
    for j in range(1, tp):
        total = total + dot(blocks[j], spread(dt, dt * tp, j * dt))
    return total


def cut(part, buffer, dt, tp):
    if dt % 128 == 0:
        for j in range(tp):
            buffer[j] = part[:, j * dt : (j + 1) * dt].astype(BF16)
    else:
        whole = part.astype(BF16)
        for j in range(tp):
            buffer[j] = dot(whole, pick(dt, dt * tp, j * dt)).astype(BF16)


def kernel(
    kv, tp, model_width,
    tokens, cosine, sine, norm_attn, norm_mlp, gain,
    memory_h, wq_h, wk_h, wv_h, wg_h, wo_h, wgm_h, wup_h, wd_h,
    result, k_out, v_out,
    memory, wq, wk, wv, wg, wo, wgm, wup, wd,
    tok_all, p32, psend, precv, sq_send, sq_recv, qpad, ro, mixed_all, m32,
    asend, arecv, mid_all, msq_send, msq_recv, f32buf, fsend, frecv, h_all, acc, dsend, drecv,
    lsem, tok_s, tok_r, sq_s, sq_r, p_s, p_r, mx_s, mx_r, a_s, a_r, md_s, md_r, ms_s, ms_r,
    f_s, f_r, h_s, h_r, d_s, d_r,
):
    z = lax.axis_index("kv")
    t = lax.axis_index("tp")
    rows, dt = tokens.shape
    own, heads, head, _ = memory.shape
    wl = heads * head
    ff = wup.shape[1]
    cw = chunk_width(ff)
    chunks = ff // cw

    local = []
    for i, (src, dst) in enumerate(
        [(wq_h, wq), (wk_h, wk), (wv_h, wv), (wg_h, wg), (memory_h, memory),
         (wo_h, wo), (wgm_h, wgm), (wup_h, wup), (wd_h, wd)]
    ):
        copy = pltpu.make_async_copy(src, dst, lsem.at[i])
        copy.start()
        local.append(copy)

    barrier = pltpu.get_barrier_semaphore()
    for d in range(1, kv):
        pl.semaphore_signal(barrier, inc=1, device_id={"kv": lax.rem(z + d, kv)}, device_id_type=MESH)
    for d in range(1, tp):
        pl.semaphore_signal(barrier, inc=1, device_id={"tp": lax.rem(t + d, tp)}, device_id_type=MESH)
    pl.semaphore_wait(barrier, kv + tp - 2)

    sends = []
    sends += start_all("tp", tp, t, lambda k: tokens, tok_all, tok_s, tok_r)
    tok_all[t] = tokens[...]
    wait_all("tp", tp, t, tok_all, tok_s, tok_r)
    tok = joined(tok_all, dt, tp)
    scaled = (tok * norm_attn[...]).astype(BF16)
    m32[:, 0:128] = jnp.broadcast_to(jnp.sum(tok * tok, axis=1, keepdims=True), (rows, 128))
    for k in range(kv):
        sq_send[k] = m32[k * own : (k + 1) * own, 0:128]
    sends += start_all("kv", kv, z, lambda k: sq_send.at[k], sq_recv, sq_s, sq_r)
    sq_recv[z] = sq_send[z]

    for i, w in enumerate((wq, wk, wv, wg)):
        local[i].wait()
        p32[:, i * wl : (i + 1) * wl] = dot(scaled, w[...])
    for k in range(kv):
        psend[k] = p32[k * own : (k + 1) * own, :].astype(BF16)
    sends += start_all("kv", kv, z, lambda k: psend.at[k], precv, p_s, p_r)
    precv[z] = psend[z]
    qpad[...] = jnp.zeros(qpad.shape, F32)
    wait_all("kv", kv, z, sq_recv, sq_s, sq_r)
    squares = sq_recv[0]
    for k in range(1, kv):
        squares = squares + sq_recv[k]
    inv = lax.rsqrt(squares / model_width + EPS)
    local[4].wait()
    wait_all("kv", kv, z, precv, p_s, p_r)

    def column(start):
        total = precv[0, :, start : start + head].astype(F32)
        for k in range(1, kv):
            total = total + precv[k, :, start : start + head].astype(F32)
        return total * inv

    cos = cosine[...]
    sin = sine[...]
    for h in range(heads):
        q = column(h * head)
        q = (q * cos + pltpu.roll(q, head // 2, 1) * sin) * head ** (-0.5)
        kk = column(wl + h * head)
        kk = kk * cos + pltpu.roll(kk, head // 2, 1) * sin
        v = column(2 * wl + h * head)
        g = column(3 * wl + h * head)
        k_out[:, h * head : (h + 1) * head] = kk
        v_out[:, h * head : (h + 1) * head] = v
        qpad[0:own, :] = q
        q_t = jnp.transpose(qpad[...])
        for b in range(own):
            ro[b : b + 1, :] = jnp.sum(memory[b, h] * q_t[:, b : b + 1], axis=0, keepdims=True)
        exponent = -5.0 - (t * heads + h).astype(F32) * (7.0 / max(HEADS - 1, 1))
        decay = 1.0 - jnp.exp2(jnp.full((1, head), exponent, F32))
        readout = decay * ro[...] + jnp.sum(q * kk, axis=1, keepdims=True) * v
        centred = readout - jnp.mean(readout, axis=1, keepdims=True)
        normed = centred * lax.rsqrt(jnp.mean(centred * centred, axis=1, keepdims=True) + EPS)
        mixed = normed * gain[:, h * head : (h + 1) * head] * (g / (1.0 + jnp.exp(-g)))
        mixed_all[z, :, h * head : (h + 1) * head] = mixed.astype(BF16)

    sends += start_all("kv", kv, z, lambda k: mixed_all.at[z], mixed_all, mx_s, mx_r)
    local[5].wait()
    wait_all("kv", kv, z, mixed_all, mx_s, mx_r)
    for k in range(kv):
        m32[k * own : (k + 1) * own, :] = mixed_all[k].astype(F32)
    cut(dot(m32[...].astype(BF16), wo[...]), asend, dt, tp)
    sends += start_all("tp", tp, t, lambda k: asend.at[k], arecv, a_s, a_r)
    arecv[t] = asend[t]
    wait_all("tp", tp, t, arecv, a_s, a_r)
    total = arecv[0].astype(F32)
    for j in range(1, tp):
        total = total + arecv[j].astype(F32)
    mid_all[t] = (tokens[...].astype(F32) + total).astype(BF16)
    sends += start_all("tp", tp, t, lambda k: mid_all.at[t], mid_all, md_s, md_r)
    local[6].wait()
    local[7].wait()
    wait_all("tp", tp, t, mid_all, md_s, md_r)
    mid = joined(mid_all, dt, tp)
    scaled = (mid * norm_mlp[...]).astype(BF16)
    m32[:, 0:128] = jnp.broadcast_to(jnp.sum(mid * mid, axis=1, keepdims=True), (rows, 128))
    for k in range(kv):
        msq_send[k] = m32[k * own : (k + 1) * own, 0:128]
    sends += start_all("kv", kv, z, lambda k: msq_send.at[k], msq_recv, ms_s, ms_r)
    msq_recv[z] = msq_send[z]

    for c in range(chunks):
        f32buf[:, 0:cw] = dot(scaled, wgm[:, c * cw : (c + 1) * cw])
        f32buf[:, cw : 2 * cw] = dot(scaled, wup[:, c * cw : (c + 1) * cw])
        for k in range(kv):
            fsend[c, k] = f32buf[k * own : (k + 1) * own, :].astype(BF16)
        sends += start_all("kv", kv, z, lambda k: fsend.at[c, k], frecv.at[c], f_s.at[c], f_r.at[c])
        frecv[c, z] = fsend[c, z]

    wait_all("kv", kv, z, msq_recv, ms_s, ms_r)
    squares = msq_recv[0]
    for k in range(1, kv):
        squares = squares + msq_recv[k]
    inv = lax.rsqrt(squares / model_width + EPS)[:, 0:1]
    for c in range(chunks):
        wait_all("kv", kv, z, frecv.at[c], f_s.at[c], f_r.at[c])
        both = frecv[c, 0].astype(F32)
        for k in range(1, kv):
            both = both + frecv[c, k].astype(F32)
        both = both * inv
        g = both[:, 0:cw]
        h_all[c, z] = (g / (1.0 + jnp.exp(-g)) * both[:, cw : 2 * cw]).astype(BF16)
        sends += start_all("kv", kv, z, lambda k: h_all.at[c, z], h_all.at[c], h_s.at[c], h_r.at[c])
    local[8].wait()
    for c in range(chunks):
        wait_all("kv", kv, z, h_all.at[c], h_s.at[c], h_r.at[c])
        for k in range(kv):
            f32buf[k * own : (k + 1) * own, 0:cw] = h_all[c, k].astype(F32)
        part = dot(f32buf[:, 0:cw].astype(BF16), wd[c * cw : (c + 1) * cw, :])
        acc[...] = part if c == 0 else acc[...] + part
    cut(acc[...], dsend, dt, tp)
    sends += start_all("tp", tp, t, lambda k: dsend.at[k], drecv, d_s, d_r)
    drecv[t] = dsend[t]
    wait_all("tp", tp, t, drecv, d_s, d_r)
    total = drecv[0].astype(F32)
    for j in range(1, tp):
        total = total + drecv[j].astype(F32)
    result[...] = (mid_all[t].astype(F32) + total).astype(BF16)
    for copy in sends:
        copy.wait_send()


def per_device(kv, tp, tokens, lengths, memory, norm_attn, w_query, w_key, w_value, w_gate,
               head_gain, w_out, norm_mlp, w_gate_mlp, w_up, w_down):
    own, heads, head, _ = memory.shape
    rows, dt = tokens.shape
    dk, wl = w_query.shape
    ff = w_up.shape[1]
    cw = chunk_width(ff)
    chunks = ff // cw
    half = head // 2
    inverse = 10000.0 ** (-jnp.arange(half, dtype=F32) / half)
    inverse = jnp.concatenate([inverse, inverse])
    angles = lengths.astype(F32)[:, None] * inverse[None, :]
    sign = jnp.where(jnp.arange(head) < half, -1.0, 1.0)[None, :]
    vm = pl.BlockSpec(memory_space=pltpu.VMEM)
    hbm = pl.BlockSpec(memory_space=pl.ANY)
    dma = pltpu.SemaphoreType.DMA
    padded = -(-own // 8) * 8

    def pair(n, *lead):
        return [dma(lead + (n - 1,)), dma(lead + (n,))]

    scratch = [
        pltpu.VMEM(memory.shape, F32),
        *[pltpu.VMEM((dk, wl), BF16)] * 4,
        pltpu.VMEM((wl, dk), BF16),
        pltpu.VMEM((dk, ff), BF16),
        pltpu.VMEM((dk, ff), BF16),
        pltpu.VMEM((ff, dk), BF16),
        pltpu.VMEM((tp, rows, dt), BF16),
        pltpu.VMEM((rows, 4 * wl), F32),
        pltpu.VMEM((kv, own, 4 * wl), BF16),
        pltpu.VMEM((kv, own, 4 * wl), BF16),
        pltpu.VMEM((kv, own, 128), F32),
        pltpu.VMEM((kv, own, 128), F32),
        pltpu.VMEM((padded, head), F32),
        pltpu.VMEM((own, head), F32),
        pltpu.VMEM((kv, own, wl), BF16),
        pltpu.VMEM((rows, wl), F32),
        pltpu.VMEM((tp, rows, dt), BF16),
        pltpu.VMEM((tp, rows, dt), BF16),
        pltpu.VMEM((tp, rows, dt), BF16),
        pltpu.VMEM((kv, own, 128), F32),
        pltpu.VMEM((kv, own, 128), F32),
        pltpu.VMEM((rows, 2 * cw), F32),
        pltpu.VMEM((chunks, kv, own, 2 * cw), BF16),
        pltpu.VMEM((chunks, kv, own, 2 * cw), BF16),
        pltpu.VMEM((chunks, kv, own, cw), BF16),
        pltpu.VMEM((rows, dk), F32),
        pltpu.VMEM((tp, rows, dt), BF16),
        pltpu.VMEM((tp, rows, dt), BF16),
        dma((9,)),
        *pair(tp), *pair(kv), *pair(kv), *pair(kv), *pair(tp), *pair(tp), *pair(kv),
        *pair(kv, chunks), *pair(kv, chunks), *pair(tp),
    ]
    result, keys, values = pl.pallas_call(
        functools.partial(kernel, kv, tp, float(dk * kv)),
        out_shape=(
            jax.ShapeDtypeStruct((rows, dt), BF16),
            jax.ShapeDtypeStruct((own, wl), F32),
            jax.ShapeDtypeStruct((own, wl), F32),
        ),
        in_specs=[vm] * 6 + [hbm] * 9,
        out_specs=(vm, vm, vm),
        scratch_shapes=scratch,
        compiler_params=pltpu.CompilerParams(
            collective_id=0, has_side_effects=True, vmem_limit_bytes=60 * 1024 * 1024
        ),
    )(
        tokens, jnp.cos(angles), jnp.sin(angles) * sign,
        norm_attn.astype(F32)[None, :], norm_mlp.astype(F32)[None, :], head_gain.astype(F32)[None, :],
        memory, w_query, w_key, w_value, w_gate, w_out, w_gate_mlp, w_up, w_down,
    )
    decay = head_decay(lax.axis_index("tp") * heads + jnp.arange(heads))
    keys = keys.reshape(own, heads, head)
    values = values.reshape(own, heads, head)
    new_memory = (
        decay[None, :, None, None] * memory + keys[:, :, :, None] * values[:, :, None, :]
    )
    return result, new_memory


def solution(mesh):
    in_specs = (
        P("grp", ("kv", "tp")),
        P(("grp", "kv")),
        P(("grp", "kv"), "tp", None, None),
        P("kv"),
        P("kv", "tp"),
        P("kv", "tp"),
        P("kv", "tp"),
        P("kv", "tp"),
        P("tp"),
        P("tp", "kv"),
        P("kv"),
        P("kv", "tp"),
        P("kv", "tp"),
        P("tp", "kv"),
    )
    out_specs = (P("grp", ("kv", "tp")), P(("grp", "kv"), "tp", None, None))
    return jax.shard_map(
        functools.partial(per_device, mesh.shape["kv"], mesh.shape["tp"]),
        mesh=mesh, in_specs=in_specs, out_specs=out_specs, check_vma=False,
    )
```

time: 205 us -> 102 us (0.50)
  blocking collectives: 108 us -> 0 us
  Pallas kernels: 0 us -> 87.1 us
  waiting for transfers between devices: 37.7 us -> 0 us
  matrix products: 25.6 us -> 0 us
  between operations: 15.1 us -> 0.66 us
  starting transfers between devices: 3.75 us -> 0 us
  local copies, waits for them, and re-layouts: 5.9 us -> 2.25 us
  other arithmetic: 8.66 us -> 11.7 us
    pallas_call x0 -> x1, Pallas kernels: none -> 87.1 us  [per_device(): pl.pallas_call(functools.partial(kernel, kv, tp, float(dk * kv)), out_sha...]
    unnamed x2 -> x0, blocking collectives: 48 us -> none
    all_gather x4 -> x0, blocking collectives: 41.1 us -> none  [the longest x1 15.4 us: per_device(): lax.all_gather(hidden, 'kv', axis=0, tiled=True)]
    reduce_scatter x2 -> x0, waiting for transfers between devices: 37.7 us -> none  [the longest x1 19.5 us: per_device(): lax.psum_scatter(attn_part.astype(jnp.bfloat16), 'tp', scatter_dimension=...]
    dot_general x9 -> x0, matrix products: 25.6 us -> none  [the longest x4 6.06 us: per_device(): jnp.dot(block_rows, weight, preferred_element_type=jnp.float32)]
    psum x2 -> x0, blocking collectives: 18.6 us -> none  [the longest x1 10.1 us: per_device(): square_sums = lax.psum(mid_squares, 'kv')]
    unnamed x23 -> x3, local copies, waits for them, and re-layouts: 5.84 us -> 0.62 us
    broadcast_in_dim x0 -> x3, other arithmetic: none -> 3.8 us  [the longest x1 1.27 us: per_device(): norm_attn.astype(F32)[None, :]]
  transfers between devices with their start and end apart: 4 -> 0, of which waited for: 2 -> 0; matrix products, arithmetic and copies ran while one was open for 1% -> 0% of each run, Pallas kernels for 0% -> 0%
where the time goes in v1:
time: 102 us
  Pallas kernels  87.1 us (85%)
  other arithmetic  11.7 us (11%)
  local copies, waits for them, and re-layouts  2.25 us (2%)
    pallas_call x1, Pallas kernels, per_device(): pl.pallas_call(functools.partial(kernel, kv, tp, float(dk * kv)), out_sha...  87.1 us
    add x1, other arithmetic, per_device(): decay[None, :, None, None] * memory  6.37 us

profile of v1, /device:TPU:0, one launch (start us, length us, event | category | flops | bytes accessed | tf_op | source)
XLA Modules:
  0.0 101.7 jit_solution(2105994457480402383)
XLA Ops:
  0.6 0.7 convert_element_type.13
  1.3 0.1 compare_select_fusion
  1.4 1.3 %broadcast_in_dim.37 = f32[512]{0:T(512)} convert(bf16[512]{0:T(512)(128)(2,1)} %param.22) | non-fusion elementwise | flops 512 | bytes 3072 | tf_op jit(solution)/shard_map/broadcast_in_dim | solution.py:319
  2.7 1.3 %broadcast_in_dim.35 = f32[1024]{0:T(1024)} convert(bf16[1024]{0:T(1024)(128)(2,1)} %param.17) | non-fusion elementwise | flops 1024 | bytes 6144 | tf_op jit(solution)/shard_map/broadcast_in_dim | solution.py:319
  3.9 1.3 %broadcast_in_dim.36 = f32[1024]{0:T(1024)} convert(bf16[1024]{0:T(1024)(128)(2,1)} %param.24) | non-fusion elementwise | flops 1024 | bytes 6144 | tf_op jit(solution)/shard_map/broadcast_in_dim | solution.py:319
  5.2 0.7 fusion
  5.9 87.1 %shard_map.149 = (bf16[80,256]{1,0:T(8,128)(2,1)}, f32[20,512]{1,0:T(8,128)}, f32[20,512]{1,0:T(8,128)}) custom-call(bf16[80,256]{1,0:T(8,128)(2,1)} %tokens.1, f32[20,128]{1,0:T(8,128)} %get-tuple-element.9.cosine, f32[20,128]{1,0:T(8,128)} %get-tuple-element.8.sine, f32[1,1024]{1,0:T(1,128)} %bitcast.3, f32[1,1024]{1,0:T(1,128)} %bitcast.4, ...), custom_call_target="tpu_custom_call" | custom-call | tf_op jit(solution)/shard_map/pallas_call | solution.py:304
  93.1 0.8 mul.65
  93.9 0.8 mul.67
  94.7 0.0 copy-start
  94.7 6.4 %multiply_add_fusion = f32[20,4,128,128]{3,2,1,0:T(8,128)} fusion(f32[20,4,128,128]{3,2,1,0:T(8,128)} %memory_h.1, f32[20,4,128]{2,1,0:T(4,128)S(1)} %mul.67, f32[20,4,128]{2,1,0:T(4,128)S(1)} %mul.65, f32[4]{0:T(128)S(1)} %exponential_subtract_fusion), kind=kLoop, calls=%fused_computation | loop fusion | flops 3932160 | bytes 10567696 | tf_op jit(solution)/shard_map/add | solution.py:326
  101.1 0.0 copy-done
  101.1 0.6 copy.17
  (2 shorter events, 0.0 us)
Async XLA Ops:
  94.7 6.4 %copy-start = (bf16[80,256]{1,0:T(8,128)(2,1)S(1)}, bf16[80,256]{1,0:T(8,128)(2,1)}, u32[]{:S(2)}) copy-start(bf16[80,256]{1,0:T(8,128)(2,1)} %get-tuple-element.14) | copy-start | bytes 122884

commit v2 on v1

--- a/solution.py
+++ b/solution.py
@@ -14,17 +14,20 @@
 MESH = pl.DeviceIdType.MESH
 
 
-def head_decay(head_index):
-    exponent = -5.0 - head_index.astype(F32) * (7.0 / max(HEADS - 1, 1))
-    return 1.0 - jnp.exp2(exponent)
-
-
 def dot(a, b):
     return jnp.dot(a, b, preferred_element_type=F32)
 
 
 def chunk_width(ff_local):
-    return 512 if ff_local % 512 == 0 else 128
+    return 256 if ff_local % 256 == 0 else 128
+
+
+SKEW = 2
+
+
+def as_row(ref):
+    parts = ref[...].astype(F32)
+    return jnp.concatenate([parts[i : i + 1] for i in range(parts.shape[0])], axis=1)
 
 
 def start_all(axis, n, me, src_of, dst, ssem, rsem):
@@ -90,14 +93,15 @@
 
 def kernel(
     kv, tp, model_width,
-    tokens, cosine, sine, norm_attn, norm_mlp, gain,
+    tokens, cosine, sine, norm_attn, norm_mlp, gain_h,
     memory_h, wq_h, wk_h, wv_h, wg_h, wo_h, wgm_h, wup_h, wd_h,
     result, k_out, v_out,
     memory, wq, wk, wv, wg, wo, wgm, wup, wd,
-    tok_all, p32, psend, precv, sq_send, sq_recv, qpad, ro, mixed_all, m32,
-    asend, arecv, mid_all, msq_send, msq_recv, f32buf, fsend, frecv, h_all, acc, dsend, drecv,
-    lsem, tok_s, tok_r, sq_s, sq_r, p_s, p_r, mx_s, mx_r, a_s, a_r, md_s, md_r, ms_s, ms_r,
-    f_s, f_r, h_s, h_r, d_s, d_r,
+    tok_all, p32, psend, precv, sq_send, sq_recv, qpad, qrot, ro, mixed_all, m32,
+    asend, arecv, mid_all, msq_send, msq_recv, inv_ref, scaled_ref,
+    part, csend, crecv, h_all, acc, dsend, drecv,
+    lsem, tok_s, tok_r, sq_s, sq_r, p_s, p_r, mx_s, mx_r, a_s, a_r, md_s, md_r, d_s, d_r,
+    ms_s, ms_r, c_s, c_r, h_s, h_r,
 ):
     z = lax.axis_index("kv")
     t = lax.axis_index("tp")
@@ -129,7 +133,7 @@
     tok_all[t] = tokens[...]
     wait_all("tp", tp, t, tok_all, tok_s, tok_r)
     tok = joined(tok_all, dt, tp)
-    scaled = (tok * norm_attn[...]).astype(BF16)
+    scaled = (tok * as_row(norm_attn)).astype(BF16)
     m32[:, 0:128] = jnp.broadcast_to(jnp.sum(tok * tok, axis=1, keepdims=True), (rows, 128))
     for k in range(kv):
         sq_send[k] = m32[k * own : (k + 1) * own, 0:128]
@@ -138,50 +142,58 @@
 
     for i, w in enumerate((wq, wk, wv, wg)):
         local[i].wait()
-        p32[:, i * wl : (i + 1) * wl] = dot(scaled, w[...])
-    for k in range(kv):
-        psend[k] = p32[k * own : (k + 1) * own, :].astype(BF16)
-    sends += start_all("kv", kv, z, lambda k: psend.at[k], precv, p_s, p_r)
-    precv[z] = psend[z]
+        p32[...] = dot(scaled, w[...])
+        for k in range(kv):
+            psend[i, k] = p32[k * own : (k + 1) * own, :].astype(BF16)
+        sends += start_all("kv", kv, z, lambda k: psend.at[i, k], precv.at[i], p_s.at[i], p_r.at[i])
+        precv[i, z] = psend[i, z]
     qpad[...] = jnp.zeros(qpad.shape, F32)
     wait_all("kv", kv, z, sq_recv, sq_s, sq_r)
     squares = sq_recv[0]
     for k in range(1, kv):
         squares = squares + sq_recv[k]
     inv = lax.rsqrt(squares / model_width + EPS)
-    local[4].wait()
-    wait_all("kv", kv, z, precv, p_s, p_r)
-
-    def column(start):
-        total = precv[0, :, start : start + head].astype(F32)
+
+    def column(i, h):
+        start = h * head
+        total = precv[i, 0, :, start : start + head].astype(F32)
         for k in range(1, kv):
-            total = total + precv[k, :, start : start + head].astype(F32)
+            total = total + precv[i, k, :, start : start + head].astype(F32)
         return total * inv
 
     cos = cosine[...]
     sin = sine[...]
+    gain = as_row(gain_h)
+    local[4].wait()
+    wait_all("kv", kv, z, precv.at[0], p_s.at[0], p_r.at[0])
     for h in range(heads):
-        q = column(h * head)
+        q = column(0, h)
         q = (q * cos + pltpu.roll(q, head // 2, 1) * sin) * head ** (-0.5)
-        kk = column(wl + h * head)
+        qrot[h] = q
+        qpad[h, 0:own, :] = q
+        q_t = jnp.transpose(qpad[h])
+        for b in range(own):
+            ro[h, b : b + 1, :] = jnp.sum(memory[b, h] * q_t[:, b : b + 1], axis=0, keepdims=True)
+    for i in (1, 2, 3):
+        wait_all("kv", kv, z, precv.at[i], p_s.at[i], p_r.at[i])
+    for h in range(heads):
+        kk = column(1, h)
         kk = kk * cos + pltpu.roll(kk, head // 2, 1) * sin
-        v = column(2 * wl + h * head)
-        g = column(3 * wl + h * head)
-        k_out[:, h * head : (h + 1) * head] = kk
+        v = column(2, h)
+        g = column(3, h)
+        qpad[h, 0:own, :] = kk
         v_out[:, h * head : (h + 1) * head] = v
-        qpad[0:own, :] = q
-        q_t = jnp.transpose(qpad[...])
-        for b in range(own):
-            ro[b : b + 1, :] = jnp.sum(memory[b, h] * q_t[:, b : b + 1], axis=0, keepdims=True)
         exponent = -5.0 - (t * heads + h).astype(F32) * (7.0 / max(HEADS - 1, 1))
         decay = 1.0 - jnp.exp2(jnp.full((1, head), exponent, F32))
-        readout = decay * ro[...] + jnp.sum(q * kk, axis=1, keepdims=True) * v
+        readout = decay * ro[h] + jnp.sum(qrot[h] * kk, axis=1, keepdims=True) * v
         centred = readout - jnp.mean(readout, axis=1, keepdims=True)
         normed = centred * lax.rsqrt(jnp.mean(centred * centred, axis=1, keepdims=True) + EPS)
         mixed = normed * gain[:, h * head : (h + 1) * head] * (g / (1.0 + jnp.exp(-g)))
         mixed_all[z, :, h * head : (h + 1) * head] = mixed.astype(BF16)
 
     sends += start_all("kv", kv, z, lambda k: mixed_all.at[z], mixed_all, mx_s, mx_r)
+    for h in range(heads):
+        k_out[h] = jnp.transpose(qpad[h])
     local[5].wait()
     wait_all("kv", kv, z, mixed_all, mx_s, mx_r)
     for k in range(kv):
@@ -199,42 +211,125 @@
     local[7].wait()
     wait_all("tp", tp, t, mid_all, md_s, md_r)
     mid = joined(mid_all, dt, tp)
-    scaled = (mid * norm_mlp[...]).astype(BF16)
-    m32[:, 0:128] = jnp.broadcast_to(jnp.sum(mid * mid, axis=1, keepdims=True), (rows, 128))
-    for k in range(kv):
-        msq_send[k] = m32[k * own : (k + 1) * own, 0:128]
-    sends += start_all("kv", kv, z, lambda k: msq_send.at[k], msq_recv, ms_s, ms_r)
-    msq_recv[z] = msq_send[z]
-
-    for c in range(chunks):
-        f32buf[:, 0:cw] = dot(scaled, wgm[:, c * cw : (c + 1) * cw])
-        f32buf[:, cw : 2 * cw] = dot(scaled, wup[:, c * cw : (c + 1) * cw])
-        for k in range(kv):
-            fsend[c, k] = f32buf[k * own : (k + 1) * own, :].astype(BF16)
-        sends += start_all("kv", kv, z, lambda k: fsend.at[c, k], frecv.at[c], f_s.at[c], f_r.at[c])
-        frecv[c, z] = fsend[c, z]
-
-    wait_all("kv", kv, z, msq_recv, ms_s, ms_r)
-    squares = msq_recv[0]
-    for k in range(1, kv):
-        squares = squares + msq_recv[k]
-    inv = lax.rsqrt(squares / model_width + EPS)[:, 0:1]
-    for c in range(chunks):
-        wait_all("kv", kv, z, frecv.at[c], f_s.at[c], f_r.at[c])
-        both = frecv[c, 0].astype(F32)
-        for k in range(1, kv):
-            both = both + frecv[c, k].astype(F32)
-        both = both * inv
-        g = both[:, 0:cw]
-        h_all[c, z] = (g / (1.0 + jnp.exp(-g)) * both[:, cw : 2 * cw]).astype(BF16)
-        sends += start_all("kv", kv, z, lambda k: h_all.at[c, z], h_all.at[c], h_s.at[c], h_r.at[c])
+    scaled = (mid * as_row(norm_mlp)).astype(BF16)
+    scaled_ref[...] = scaled
+    mid_squares = jnp.broadcast_to(jnp.sum(mid * mid, axis=1, keepdims=True), (rows, 128))
+    half = rows // 2
+    last = kv - 1
+    places = (z == 0, z == last)
+    ends = (0, last)
+    for side in (0, 1):
+        msq_send[side] = mid_squares[side * half : (side + 1) * half]
+
+    def squares_copy(side, sender):
+        return pltpu.make_async_remote_copy(
+            src_ref=msq_send.at[side],
+            dst_ref=msq_recv.at[sender],
+            send_sem=ms_s.at[side],
+            recv_sem=ms_r.at[sender],
+            device_id={"kv": ends[side]},
+            device_id_type=MESH,
+        )
+
+    for side in (0, 1):
+        @pl.when(jnp.logical_not(places[side]))
+        def _():
+            squares_copy(side, z).start()
+
+    onward = (lax.rem(z + last, kv), lax.rem(z + 1, kv))
+    depth = (last - z, z)
+
+    def chain_copy(side, c):
+        return pltpu.make_async_remote_copy(
+            src_ref=csend.at[side, c],
+            dst_ref=crecv.at[side, c],
+            send_sem=c_s.at[side, c],
+            recv_sem=c_r.at[side, c],
+            device_id={"kv": onward[side]},
+            device_id_type=MESH,
+        )
+
+    def hidden_copy(side, c):
+        return pltpu.make_async_remote_copy(
+            src_ref=h_all.at[side, c],
+            dst_ref=h_all.at[side, c],
+            send_sem=h_s.at[side, c],
+            recv_sem=h_r.at[side, c],
+            device_id={"kv": onward[1 - side]},
+            device_id_type=MESH,
+        )
+
+    def within(c):
+        return jnp.logical_and(c >= 0, c < chunks)
+
+    acc[...] = jnp.zeros(acc.shape, F32)
     local[8].wait()
-    for c in range(chunks):
-        wait_all("kv", kv, z, h_all.at[c], h_s.at[c], h_r.at[c])
-        for k in range(kv):
-            f32buf[k * own : (k + 1) * own, 0:cw] = h_all[c, k].astype(F32)
-        part = dot(f32buf[:, 0:cw].astype(BF16), wd[c * cw : (c + 1) * cw, :])
-        acc[...] = part if c == 0 else acc[...] + part
+    full = SKEW * last
+
+    def step(s, carry):
+        @pl.when(s < chunks)
+        def _():
+            cols = pl.ds(pl.multiple_of(s * cw, cw), cw)
+            lhs = scaled_ref[...]
+            g = dot(lhs, wgm[:, cols])
+            u = dot(lhs, wup[:, cols])
+            for side in (0, 1):
+                part[s, side, :, 0:cw] = g[side * half : (side + 1) * half]
+                part[s, side, :, cw : 2 * cw] = u[side * half : (side + 1) * half]
+
+        for side in (0, 1):
+            c = s - SKEW * depth[side]
+
+            @pl.when(jnp.logical_and(within(c), depth[side] == 0))
+            def _():
+                csend[side, c] = part[c, side].astype(BF16)
+                chain_copy(side, c).start()
+
+            @pl.when(jnp.logical_and(within(c), jnp.logical_and(depth[side] > 0, depth[side] < last)))
+            def _():
+                chain_copy(side, c).wait_recv()
+                csend[side, c] = (part[c, side] + crecv[side, c].astype(F32)).astype(BF16)
+                chain_copy(side, c).start()
+
+            @pl.when(jnp.logical_and(within(c), depth[side] == last))
+            def _():
+                @pl.when(c == 0)
+                def _():
+                    squares = msq_send[side]
+                    for d in range(1, kv):
+                        sender = d if side == 0 else last - d
+                        squares_copy(side, sender).wait_recv()
+                        squares = squares + msq_recv[sender]
+                    inv_ref[...] = lax.rsqrt(squares / model_width + EPS)
+
+                chain_copy(side, c).wait_recv()
+                both = (part[c, side] + crecv[side, c].astype(F32)) * inv_ref[:, 0:1]
+                g = both[:, 0:cw]
+                h_all[side, c] = (g / (1.0 + jnp.exp(-g)) * both[:, cw : 2 * cw]).astype(BF16)
+                hidden_copy(side, c).start()
+
+        for side in (0, 1):
+            behind = depth[1 - side]
+            c = s - full - SKEW * behind
+
+            @pl.when(jnp.logical_and(within(c), behind > 0))
+            def _():
+                hidden_copy(side, c).wait_recv()
+
+                @pl.when(behind < last)
+                def _():
+                    hidden_copy(side, c).start()
+
+        c = s - full - SKEW * jnp.maximum(depth[0], depth[1])
+
+        @pl.when(within(c))
+        def _():
+            lhs = jnp.concatenate([h_all[0, c].astype(F32), h_all[1, c].astype(F32)], axis=0)
+            acc[...] += dot(lhs.astype(BF16), wd[pl.ds(pl.multiple_of(c * cw, cw), cw), :])
+
+        return carry
+
+    lax.fori_loop(0, chunks + 2 * full, step, 0)
     cut(acc[...], dsend, dt, tp)
     sends += start_all("tp", tp, t, lambda k: dsend.at[k], drecv, d_s, d_r)
     drecv[t] = dsend[t]
@@ -245,6 +340,42 @@
     result[...] = (mid_all[t].astype(F32) + total).astype(BF16)
     for copy in sends:
         copy.wait_send()
+    for side in (0, 1):
+        @pl.when(jnp.logical_not(places[side]))
+        def _():
+            squares_copy(side, z).wait_send()
+
+    def drain(c, carry):
+        for side in (0, 1):
+            @pl.when(depth[side] < last)
+            def _():
+                chain_copy(side, c).wait_send()
+
+            @pl.when(depth[1 - side] < last)
+            def _():
+                hidden_copy(side, c).wait_send()
+        return carry
+
+    lax.fori_loop(0, chunks, drain, 0)
+
+
+def state_kernel(memory_h, keys, values, out_h, held, made, in_sem, out_sem):
+    own, heads, head, _ = held.shape
+    first = lax.axis_index("tp") * heads
+    reads = [pltpu.make_async_copy(memory_h.at[b], held.at[b], in_sem.at[b]) for b in range(own)]
+    writes = [pltpu.make_async_copy(made.at[b], out_h.at[b], out_sem.at[b]) for b in range(own)]
+    for copy in reads:
+        copy.start()
+    for b in range(own):
+        reads[b].wait()
+        for h in range(heads):
+            exponent = -5.0 - (first + h).astype(F32) * (7.0 / max(HEADS - 1, 1))
+            decay = 1.0 - jnp.exp2(jnp.full((1, head), exponent, F32))
+            row = values[b : b + 1, h * head : (h + 1) * head]
+            made[b, h] = decay * held[b, h] + keys[h, :, b : b + 1] * row
+        writes[b].start()
+    for copy in writes:
+        copy.wait()
 
 
 def per_device(kv, tp, tokens, lengths, memory, norm_attn, w_query, w_key, w_value, w_gate,
@@ -276,36 +407,39 @@
         pltpu.VMEM((dk, ff), BF16),
         pltpu.VMEM((ff, dk), BF16),
         pltpu.VMEM((tp, rows, dt), BF16),
-        pltpu.VMEM((rows, 4 * wl), F32),
-        pltpu.VMEM((kv, own, 4 * wl), BF16),
-        pltpu.VMEM((kv, own, 4 * wl), BF16),
+        pltpu.VMEM((rows, wl), F32),
+        pltpu.VMEM((4, kv, own, wl), BF16),
+        pltpu.VMEM((4, kv, own, wl), BF16),
         pltpu.VMEM((kv, own, 128), F32),
         pltpu.VMEM((kv, own, 128), F32),
-        pltpu.VMEM((padded, head), F32),
-        pltpu.VMEM((own, head), F32),
+        pltpu.VMEM((heads, padded, head), F32),
+        pltpu.VMEM((heads, own, head), F32),
+        pltpu.VMEM((heads, own, head), F32),
         pltpu.VMEM((kv, own, wl), BF16),
         pltpu.VMEM((rows, wl), F32),
         pltpu.VMEM((tp, rows, dt), BF16),
         pltpu.VMEM((tp, rows, dt), BF16),
         pltpu.VMEM((tp, rows, dt), BF16),
-        pltpu.VMEM((kv, own, 128), F32),
-        pltpu.VMEM((kv, own, 128), F32),
-        pltpu.VMEM((rows, 2 * cw), F32),
-        pltpu.VMEM((chunks, kv, own, 2 * cw), BF16),
-        pltpu.VMEM((chunks, kv, own, 2 * cw), BF16),
-        pltpu.VMEM((chunks, kv, own, cw), BF16),
+        pltpu.VMEM((2, rows // 2, 128), F32),
+        pltpu.VMEM((kv, rows // 2, 128), F32),
+        pltpu.VMEM((rows // 2, 128), F32),
+        pltpu.VMEM((rows, dk), BF16),
+        pltpu.VMEM((chunks, 2, rows // 2, 2 * cw), F32),
+        pltpu.VMEM((2, chunks, rows // 2, 2 * cw), BF16),
+        pltpu.VMEM((2, chunks, rows // 2, 2 * cw), BF16),
+        pltpu.VMEM((2, chunks, rows // 2, cw), BF16),
         pltpu.VMEM((rows, dk), F32),
         pltpu.VMEM((tp, rows, dt), BF16),
         pltpu.VMEM((tp, rows, dt), BF16),
         dma((9,)),
-        *pair(tp), *pair(kv), *pair(kv), *pair(kv), *pair(tp), *pair(tp), *pair(kv),
-        *pair(kv, chunks), *pair(kv, chunks), *pair(tp),
+        *pair(tp), *pair(kv), *pair(kv, 4), *pair(kv), *pair(tp), *pair(tp), *pair(tp),
+        dma((2,)), dma((kv,)), *[dma((2, chunks))] * 4,
     ]
     result, keys, values = pl.pallas_call(
         functools.partial(kernel, kv, tp, float(dk * kv)),
         out_shape=(
             jax.ShapeDtypeStruct((rows, dt), BF16),
-            jax.ShapeDtypeStruct((own, wl), F32),
+            jax.ShapeDtypeStruct((heads, head, padded), F32),
             jax.ShapeDtypeStruct((own, wl), F32),
         ),
         in_specs=[vm] * 6 + [hbm] * 9,
@@ -316,15 +450,17 @@
         ),
     )(
         tokens, jnp.cos(angles), jnp.sin(angles) * sign,
-        norm_attn.astype(F32)[None, :], norm_mlp.astype(F32)[None, :], head_gain.astype(F32)[None, :],
+        norm_attn.reshape(-1, 128), norm_mlp.reshape(-1, 128), head_gain.reshape(-1, 128),
         memory, w_query, w_key, w_value, w_gate, w_out, w_gate_mlp, w_up, w_down,
     )
-    decay = head_decay(lax.axis_index("tp") * heads + jnp.arange(heads))
-    keys = keys.reshape(own, heads, head)
-    values = values.reshape(own, heads, head)
-    new_memory = (
-        decay[None, :, None, None] * memory + keys[:, :, :, None] * values[:, :, None, :]
-    )
+    new_memory = pl.pallas_call(
+        state_kernel,
+        out_shape=jax.ShapeDtypeStruct(memory.shape, F32),
+        in_specs=[hbm, vm, vm],
+        out_specs=hbm,
+        scratch_shapes=[pltpu.VMEM(memory.shape, F32), pltpu.VMEM(memory.shape, F32), dma((own,)), dma((own,))],
+        compiler_params=pltpu.CompilerParams(vmem_limit_bytes=40 * 1024 * 1024),
+    )(memory, keys, values)
     return result, new_memory
 
 

time: 102 us -> 87.8 us (0.86)
  other arithmetic: 11.7 us -> 1.48 us
  Pallas kernels: 87.1 us -> 80.5 us
  local copies, waits for them, and re-layouts: 2.25 us -> 4.85 us
    pallas_call x1, Pallas kernels: 87.1 us -> 76.3 us  [per_device(): pl.pallas_call(functools.partial(kernel, kv, tp, float(dk * kv)), out_sha...]
    add x1 -> x0, other arithmetic: 6.37 us -> none  [per_device(): decay[None, :, None, None] * memory]
    unnamed x3 -> x9, local copies, waits for them, and re-layouts: 0.62 us -> 4.85 us
    pallas_call x0 -> x1, Pallas kernels: none -> 4.18 us  [per_device(): pl.pallas_call(state_kernel, out_shape=jax.ShapeDtypeStruct(memory.shape,...]
    broadcast_in_dim x3 -> x0, other arithmetic: 3.8 us -> none  [the longest x1 1.27 us: per_device(): norm_attn.astype(F32)[None, :]]
    mul x2 -> x0, local copies, waits for them, and re-layouts: 1.63 us -> none  [per_device(): keys[:, :, :, None] * values[:, :, None, :]]
where the time goes in v2:
time: 87.8 us; the launch traced here: 87.5 us
  Pallas kernels  80.5 us (92%)
  local copies, waits for them, and re-layouts  4.85 us (6%)
  other arithmetic  1.48 us (2%)
    pallas_call x1, Pallas kernels, per_device(): pl.pallas_call(functools.partial(kernel, kv, tp, float(dk * kv)), out_sha...  76.3 us
    unnamed x9, local copies, waits for them, and re-layouts  4.85 us
    pallas_call x1, Pallas kernels, per_device(): pl.pallas_call(state_kernel, out_shape=jax.ShapeDtypeStruct(memory.shape,...  4.18 us

profile of v2, /device:TPU:0, one launch (start us, length us, event | category | flops | bytes accessed | tf_op | source)
XLA Modules:
  0.0 87.5 jit_solution(14988386112180601761)
XLA Ops:
  0.6 0.7 convert_element_type.3
  1.3 0.1 compare_select_fusion
  1.4 0.7 fusion
  2.1 76.3 %shard_map.149 = (bf16[80,256]{1,0:T(8,128)(2,1)}, f32[4,128,24]{2,1,0:T(8,128)}, f32[20,512]{1,0:T(8,128)}) custom-call(bf16[80,256]{1,0:T(8,128)(2,1)} %tokens.1, f32[20,128]{1,0:T(8,128)} %get-tuple-element.9.cosine, f32[20,128]{1,0:T(8,128)} %get-tuple-element.8.sine, bf16[8,128]{1,0:T(8,128)(2,1)} %bitcast.3, bf16[8,128]{1,0:T(8,128)(2,1)} %bitcast.4, ...), custom_call_target="tpu_custom_call" | custom-call | tf_op jit(solution)/shard_map/pallas_call | solution.py:438
  78.5 0.0 copy-start
  78.5 2.5 %copy-done = f32[20,4,128,128]{3,2,1,0:T(8,128)S(1)} copy-done((f32[20,4,128,128]{3,2,1,0:T(8,128)S(1)}, f32[20,4,128,128]{3,2,1,0:T(8,128)}, u32[]{:S(2)}) %copy-start) | copy-done | bytes 5242904
  80.9 0.0 copy-start.1
  80.9 0.9 %copy-done.1 = f32[4,128,24]{2,1,0:T(8,128)S(1)} copy-done((f32[4,128,24]{2,1,0:T(8,128)S(1)}, f32[4,128,24]{2,1,0:T(8,128)}, u32[]{:S(2)}) %copy-start.1) | copy-done | bytes 49176
  81.9 0.0 copy-start.2
  81.9 0.8 copy-done.2
  82.7 0.0 copy-start.3
  82.7 4.2 %shard_map.150 = f32[20,4,128,128]{3,2,1,0:T(8,128)} custom-call(f32[20,4,128,128]{3,2,1,0:T(8,128)S(1)} %copy-done, f32[4,128,24]{2,1,0:T(8,128)S(1)} %copy-done.1, f32[20,512]{1,0:T(8,128)S(1)} %copy-done.2), custom_call_target="tpu_custom_call" | custom-call | tf_op jit(solution)/shard_map/pallas_call | solution.py:456
  86.9 0.0 copy-done.3
  86.9 0.6 copy.17
  (1 shorter events, 0.0 us)
Async XLA Ops:
  78.5 2.5 %copy-start = (f32[20,4,128,128]{3,2,1,0:T(8,128)S(1)}, f32[20,4,128,128]{3,2,1,0:T(8,128)}, u32[]{:S(2)}) copy-start(f32[20,4,128,128]{3,2,1,0:T(8,128)} %memory_h.3) | copy-start | bytes 15728644
  80.9 0.9 %copy-start.1 = (f32[4,128,24]{2,1,0:T(8,128)S(1)}, f32[4,128,24]{2,1,0:T(8,128)}, u32[]{:S(2)}) copy-start(f32[4,128,24]{2,1,0:T(8,128)} %get-tuple-element.6.keys) | copy-start | bytes 147460
  81.9 0.8 copy-start.2
  82.7 4.2 %copy-start.3 = (bf16[80,256]{1,0:T(8,128)(2,1)S(1)}, bf16[80,256]{1,0:T(8,128)(2,1)}, u32[]{:S(2)}) copy-start(bf16[80,256]{1,0:T(8,128)(2,1)} %get-tuple-element.14) | copy-start | bytes 122884

commit v3 on v2

--- a/solution.py
+++ b/solution.py
@@ -19,7 +19,7 @@
 
 
 def chunk_width(ff_local):
-    return 256 if ff_local % 256 == 0 else 128
+    return 512 if ff_local % 512 == 0 else 128
 
 
 SKEW = 2
@@ -359,20 +359,25 @@
     lax.fori_loop(0, chunks, drain, 0)
 
 
-def state_kernel(memory_h, keys, values, out_h, held, made, in_sem, out_sem):
+def state_kernel(memory_h, keys_h, values_h, out_h, held, made, keys, values, in_sem, out_sem, kv_sem):
     own, heads, head, _ = held.shape
     first = lax.axis_index("tp") * heads
     reads = [pltpu.make_async_copy(memory_h.at[b], held.at[b], in_sem.at[b]) for b in range(own)]
     writes = [pltpu.make_async_copy(made.at[b], out_h.at[b], out_sem.at[b]) for b in range(own)]
-    for copy in reads:
+    rows = [pltpu.make_async_copy(keys_h, keys, kv_sem.at[0]), pltpu.make_async_copy(values_h, values, kv_sem.at[1])]
+    for copy in rows + reads:
         copy.start()
+    decays = []
+    for h in range(heads):
+        exponent = -5.0 - (first + h).astype(F32) * (7.0 / max(HEADS - 1, 1))
+        decays.append(1.0 - jnp.exp2(jnp.full((1, head), exponent, F32)))
+    for copy in rows:
+        copy.wait()
     for b in range(own):
         reads[b].wait()
         for h in range(heads):
-            exponent = -5.0 - (first + h).astype(F32) * (7.0 / max(HEADS - 1, 1))
-            decay = 1.0 - jnp.exp2(jnp.full((1, head), exponent, F32))
             row = values[b : b + 1, h * head : (h + 1) * head]
-            made[b, h] = decay * held[b, h] + keys[h, :, b : b + 1] * row
+            made[b, h] = decays[h] * held[b, h] + keys[h, :, b : b + 1] * row
         writes[b].start()
     for copy in writes:
         copy.wait()
@@ -456,10 +461,14 @@
     new_memory = pl.pallas_call(
         state_kernel,
         out_shape=jax.ShapeDtypeStruct(memory.shape, F32),
-        in_specs=[hbm, vm, vm],
+        in_specs=[hbm, hbm, hbm],
         out_specs=hbm,
-        scratch_shapes=[pltpu.VMEM(memory.shape, F32), pltpu.VMEM(memory.shape, F32), dma((own,)), dma((own,))],
-        compiler_params=pltpu.CompilerParams(vmem_limit_bytes=40 * 1024 * 1024),
+        scratch_shapes=[
+            pltpu.VMEM(memory.shape, F32), pltpu.VMEM(memory.shape, F32),
+            pltpu.VMEM(keys.shape, F32), pltpu.VMEM(values.shape, F32),
+            dma((own,)), dma((own,)), dma((2,)),
+        ],
+        compiler_params=pltpu.CompilerParams(vmem_limit_bytes=63 * 1024 * 1024),
     )(memory, keys, values)
     return result, new_memory
 

time: 87.8 us -> 79.8 us (0.909)
  local copies, waits for them, and re-layouts: 4.85 us -> 0.62 us
  Pallas kernels: 80.5 us -> 76.8 us
    pallas_call x1, Pallas kernels: 76.3 us -> 70.6 us  [per_device(): pl.pallas_call(functools.partial(kernel, kv, tp, float(dk * kv)), out_sha...]
    unnamed x9 -> x3, local copies, waits for them, and re-layouts: 4.85 us -> 0.62 us
    pallas_call x1, Pallas kernels: 4.18 us -> 6.24 us  [per_device(): pl.pallas_call(state_kernel, out_shape=jax.ShapeDtypeStruct(memory.shape,...]
where the time goes in v3:
time: 79.8 us; the launch traced here: 79.6 us
  Pallas kernels  76.8 us (96%)
  other arithmetic  1.48 us (2%)
    pallas_call x1, Pallas kernels, per_device(): pl.pallas_call(functools.partial(kernel, kv, tp, float(dk * kv)), out_sha...  70.6 us
    pallas_call x1, Pallas kernels, per_device(): pl.pallas_call(state_kernel, out_shape=jax.ShapeDtypeStruct(memory.shape,...  6.24 us

profile of v3, /device:TPU:0, one launch (start us, length us, event | category | flops | bytes accessed | tf_op | source)
XLA Modules:
  0.0 79.6 jit_solution(3310346257421326339)
XLA Ops:
  0.6 0.7 convert_element_type.3
  1.3 0.1 compare_select_fusion
  1.4 0.7 fusion
  2.1 70.6 %shard_map.149 = (bf16[80,256]{1,0:T(8,128)(2,1)}, f32[4,128,24]{2,1,0:T(8,128)}, f32[20,512]{1,0:T(8,128)}) custom-call(bf16[80,256]{1,0:T(8,128)(2,1)} %tokens.1, f32[20,128]{1,0:T(8,128)} %get-tuple-element.9.cosine, f32[20,128]{1,0:T(8,128)} %get-tuple-element.8.sine, bf16[8,128]{1,0:T(8,128)(2,1)} %bitcast.3, bf16[8,128]{1,0:T(8,128)(2,1)} %bitcast.4, ...), custom_call_target="tpu_custom_call" | custom-call | tf_op jit(solution)/shard_map/pallas_call | solution.py:443
  72.7 0.0 copy-start
  72.7 6.2 %shard_map.150 = f32[20,4,128,128]{3,2,1,0:T(8,128)} custom-call(f32[20,4,128,128]{3,2,1,0:T(8,128)} %memory_h.3, f32[4,128,24]{2,1,0:T(8,128)} %get-tuple-element.6.keys_h, f32[20,512]{1,0:T(8,128)} %get-tuple-element.7.values_h), custom_call_target="tpu_custom_call" | custom-call | tf_op jit(solution)/shard_map/pallas_call | solution.py:461
  79.0 0.0 copy-done
  79.0 0.6 copy.17
  (1 shorter events, 0.0 us)
Async XLA Ops:
  72.7 6.3 %copy-start = (bf16[80,256]{1,0:T(8,128)(2,1)S(1)}, bf16[80,256]{1,0:T(8,128)(2,1)}, u32[]{:S(2)}) copy-start(bf16[80,256]{1,0:T(8,128)(2,1)} %get-tuple-element.14) | copy-start | bytes 122884
